TPU v7x, 32 devices: a whole 2x2x4 slice. The times are simulated.
32 devices in a mesh: grp: 2 (over x), ep: 16 (over z, y, core).
Axes of the slice: x: 2, y: 2, z: 4, core: 2. Of those that a mesh axis runs over, the one named last changes fastest.
Arguments:
- queries: bfloat16 [32, 8, 128], P(('grp', 'ep')), parts along dimension 0, may hold values from -400 to 400
- fresh_token_key: bfloat16 [32, 2, 128], P(('grp', 'ep')), parts along dimension 0, may hold values from -6 to 6
- value_new: bfloat16 [32, 2, 128], P(('grp', 'ep')), parts along dimension 0, may hold values from -6 to 6
- forget_logit: float32 [32, 8], P(('grp', 'ep')), parts along dimension 0, may hold values from -8 to 8
- cache_keys: bfloat16 [32, 2, 4096, 128], P(('grp', 'ep')), parts along dimension 0, may hold values from -12 to 12
- cache_values: bfloat16 [32, 2, 4096, 128], P(('grp', 'ep')), parts along dimension 0, may hold values from -6 to 6
- cache_cumlog: float32 [32, 8, 4096], P(('grp', 'ep')), parts along dimension 0, may hold values from -572 to 0
- lengths: int32 [32], P(('grp', 'ep')), parts along dimension 0, may hold values from 1024 to 4096
- residual: bfloat16 [32, 2048], P('grp', 'ep'), parts along dimension 0, may hold values from -6 to 6
- out_weight: bfloat16 [1024, 2048], P(None, 'ep'), may hold values from -0.1875 to 0.1875
- norm_gain: float32 [2048], replicated, may hold values from 0.1 to 1.9
- expert_gate: bfloat16 [16, 704, 2048], P('ep'), may hold values from -0.125 to 0.125
- expert_up: bfloat16 [16, 704, 2048], P('ep'), may hold values from -0.125 to 0.125
- expert_down: bfloat16 [16, 704, 2048], P('ep'), may hold values from -0.21875 to 0.21875
- shared_gate: bfloat16 [1408, 2048], P('ep'), may hold values from -0.125 to 0.125
- shared_up: bfloat16 [1408, 2048], P('ep'), may hold values from -0.125 to 0.125
- shared_down: bfloat16 [1408, 2048], P(None, 'ep'), may hold values from -0.15625 to 0.15625
- routes: int32 [32, 6], P('grp'), parts along dimension 0, may hold values from 0 to 15, all different within a row; in each aligned block of 16 rows (0 to 15, 16 to 31, ...) at most 12 rows name the same one
- route_scores: float32 [32, 6], P('grp'), parts along dimension 0, may hold values from 0.05 to 1
Outputs:
- updated: bfloat16 [32, 2048], P('grp', 'ep'), parts along dimension 0
There are 2 independent parts, one for each index of `grp`. A program takes and returns all parts, laid end to end along the dimension named above; an argument that names none is the same for every part. Nothing has to cross between parts.
Inputs may be any that keep to these rules, and one draw needn't show every extreme that they name: `routes`: each row names 6 different experts; no expert is named by more than 12 rows of a part, a bound that some block reaches.
All inputs are finite; a program needn't handle non-finite values.
Results may differ from a plain program's by a relative error of at most 0.0068.
Values may be sent and summed in bfloat16 or wider, within the bound.
A program may use at most 64 MiB of HBM per device.

v0:
```python
import functools

import jax
import jax.numpy as jnp
from jax import lax
from jax.experimental import pallas as pl
from jax.experimental.pallas import tpu as pltpu
from jax.sharding import PartitionSpec as P

norm_eps = 1e-06
routed_scale = 2.5
contract_last = (((1,), (1,)), ((), ()))
LANES = 128
VMEM_LIMIT = 67043328
f32 = jnp.float32
bf16 = jnp.bfloat16


def dot_t(a, b):
    return lax.dot_general(a, b, contract_last, preferred_element_type=f32)


def join_lanes(blocks, width):
    if width % LANES == 0:
        return jnp.concatenate([b.astype(bf16) for b in blocks], axis=1)
    rows = blocks[0].shape[0]
    total = len(blocks) * width
    lane = lax.broadcasted_iota(jnp.int32, (rows, LANES), 1)
    pieces = [jnp.zeros((rows, LANES), f32) for _ in range(-(-total // LANES))]
    for k, block in enumerate(blocks):
        at, shift = divmod(k * width, LANES)
        moved = jnp.where(lane < width, block.astype(f32), 0.0)
        if shift:
            moved = pltpu.roll(moved, shift, 1)
        if shift + width <= LANES:
            pieces[at] = pieces[at] + moved
        else:
            pieces[at] = pieces[at] + jnp.where(lane >= shift, moved, 0.0)
            pieces[at + 1] = pieces[at + 1] + jnp.where(lane < shift, moved, 0.0)
    return jnp.concatenate([p.astype(bf16) for p in pieces], axis=1)[:, :total]


def widen(block):
    rows, width = block.shape
    short = -width % LANES
    if not short:
        return block
    return jnp.concatenate([block, jnp.zeros((rows, short), block.dtype)], axis=1)


def layer(
    n,
    lengths_ref,
    q_hbm,
    fresh_hbm,
    vnew_hbm,
    forget_hbm,
    residual_hbm,
    gain_hbm,
    routes_hbm,
    route_scores_hbm,
    keys_hbm,
    values_hbm,
    cumlog_hbm,
    out_w_hbm,
    gate_hbm,
    up_hbm,
    down_hbm,
    sgate_hbm,
    sup_hbm,
    sdown_hbm,
    out_ref,
    q_ref,
    fresh_ref,
    vnew_ref,
    forget_ref,
    residual_ref,
    gain_ref,
    routes_ref,
    route_scores_ref,
    keys,
    values,
    cumlog,
    out_w,
    gate_w,
    up_w,
    down_w,
    sgate_w,
    sup_w,
    sdown_w,
    scores,
    att_buf,
    att_wide,
    stream_buf,
    mid_buf,
    eo_src,
    eo_buf,
    small_sem,
    load_sem,
    key_sem,
    value_sem,
    send_sem,
    recv_sem,
):
    me = lax.axis_index("ep")
    heads, head_size = q_ref.shape[1:]
    key_heads, span = keys.shape[:2]
    groups = heads // key_heads
    rows, width = residual_ref.shape
    model = gate_w.shape[1]
    shared_width = sgate_w.shape[0]
    chunks = key_sem.shape[0]
    chunk = span // chunks

    def key_copy(c):
        part = pl.ds(c * chunk, chunk)
        return pltpu.make_async_copy(keys_hbm.at[0, :, part], keys.at[:, part], key_sem.at[c])

    def value_copy(c):
        part = pl.ds(c * chunk, chunk)
        return pltpu.make_async_copy(values_hbm.at[0, :, part], values.at[:, part], value_sem.at[c])

    cumlog_copy = pltpu.make_async_copy(cumlog_hbm.at[0], cumlog, load_sem.at[0])
    out_w_copy = pltpu.make_async_copy(out_w_hbm, out_w, load_sem.at[1])
    sgate_copy = pltpu.make_async_copy(sgate_hbm, sgate_w, load_sem.at[2])
    sup_copy = pltpu.make_async_copy(sup_hbm, sup_w, load_sem.at[3])
    gate_copy = pltpu.make_async_copy(gate_hbm.at[0], gate_w, load_sem.at[4])
    up_copy = pltpu.make_async_copy(up_hbm.at[0], up_w, load_sem.at[5])
    down_copy = pltpu.make_async_copy(down_hbm.at[0], down_w, load_sem.at[6])
    sdown_copy = pltpu.make_async_copy(sdown_hbm, sdown_w, load_sem.at[7])

    smalls = [
        pltpu.make_async_copy(src, dst, small_sem.at[i])
        for i, (src, dst) in enumerate(
            (
                (q_hbm, q_ref),
                (fresh_hbm, fresh_ref),
                (vnew_hbm, vnew_ref),
                (forget_hbm, forget_ref),
                (routes_hbm, routes_ref),
                (route_scores_hbm, route_scores_ref),
                (residual_hbm, residual_ref),
                (gain_hbm, gain_ref),
            )
        )
    ]
    for copy in smalls[:4]:
        copy.start()
    cumlog_copy.start()
    for c in range(chunks):
        key_copy(c).start()
    for c in range(chunks):
        value_copy(c).start()
    for copy in smalls[4:]:
        copy.start()
    out_w_copy.start()

    barrier = pltpu.get_barrier_semaphore()

    def greet(i, carry):
        pl.semaphore_signal(barrier, inc=1, device_id={"ep": lax.rem(me + i, n)})
        return carry

    lax.fori_loop(1, n, greet, 0)

    def remote(phase, src, dst, peer, slot):
        return pltpu.make_async_remote_copy(
            src_ref=src,
            dst_ref=dst,
            send_sem=send_sem.at[phase, peer],
            recv_sem=recv_sem.at[phase, slot],
            device_id={"ep": peer},
        )

    wide = max(width, 2 * LANES)
    per = wide // width
    turns = model // wide
    home = me // per
    toward = 1 - 2 * (home // (turns // 2))

    def visit(i):
        return lax.rem(home + toward * i + turns, turns)

    def spread(phase, buf):
        def one(i, carry):
            peer = lax.rem(me + toward * (n - i) + n, n)
            remote(phase, buf.at[me], buf.at[me], peer, me).start()
            return carry

        lax.fori_loop(1, n, one, 0)

    def arrive(phase, buf):
        def one(i, carry):
            peer = lax.rem(me + i, n)
            remote(phase, buf.at[peer], buf.at[peer], peer, peer).wait_recv()
            return carry

        lax.fori_loop(1, n, one, 0)

    def sent(phase, buf):
        def one(i, carry):
            peer = lax.rem(me + i, n)
            remote(phase, buf.at[peer], buf.at[peer], peer, peer).wait_send()
            return carry

        lax.fori_loop(1, n, one, 0)

    for copy in smalls[:4]:
        copy.wait()
    inv_root = head_size ** (-0.5)
    length = lengths_ref[0]
    q = q_ref[0]
    head_row = lax.broadcasted_iota(jnp.int32, (heads, head_size), 0)
    q_wide = jnp.concatenate(
        [jnp.where(head_row // groups == k, q, jnp.zeros_like(q)) for k in range(key_heads)], axis=1
    )
    fresh, vnew = fresh_ref[0].astype(f32), vnew_ref[0].astype(f32)
    own_key, own_value = fresh[0:1], vnew[0:1]
    for k in range(1, key_heads):
        own_key = jnp.where(head_row // groups == k, fresh[k : k + 1], own_key)
        own_value = jnp.where(head_row // groups == k, vnew[k : k + 1], own_value)
    own_score = jnp.sum(q.astype(f32) * own_key, axis=1, keepdims=True) * inv_root
    eye = lax.broadcasted_iota(jnp.int32, (heads, heads), 0) == lax.broadcasted_iota(
        jnp.int32, (heads, heads), 1
    )
    forget = jnp.sum(jnp.where(eye, forget_ref[...], 0.0), axis=1, keepdims=True)
    log_gate = jnp.minimum(forget, 0.0) - jnp.log1p(jnp.exp(-jnp.abs(forget)))

    cumlog_copy.wait()
    position = lax.broadcasted_iota(jnp.int32, (heads, span), 1)
    latest = (
        jnp.sum(jnp.where(position == length - 1, cumlog[...], 0.0), axis=1, keepdims=True)
        + log_gate
    )
    place = lax.broadcasted_iota(jnp.int32, (heads, chunk), 1)
    top = own_score
    for c in range(chunks):
        key_copy(c).wait()
        part = slice(c * chunk, (c + 1) * chunk)
        both = jnp.concatenate([keys[k, part] for k in range(key_heads)], axis=1)
        score = dot_t(q_wide, both) * inv_root + latest - cumlog[:, part]
        score = jnp.where(place + c * chunk < length, score, -jnp.inf)
        scores[:, part] = score
        top = jnp.maximum(top, jnp.max(score, axis=1, keepdims=True))

    sgate_copy.start()
    sup_copy.start()
    gate_copy.start()
    up_copy.start()
    down_copy.start()
    sdown_copy.start()

    own_weight = jnp.exp(own_score - top)
    denominator = own_weight
    weighted = jnp.zeros((heads, key_heads * head_size), f32)
    for c in range(chunks):
        value_copy(c).wait()
        part = slice(c * chunk, (c + 1) * chunk)
        weight = jnp.exp(scores[:, part] - top)
        denominator = denominator + jnp.sum(weight, axis=1, keepdims=True)
        both = jnp.concatenate([values[k, part] for k in range(key_heads)], axis=1)
        weighted = weighted + jnp.dot(weight.astype(bf16), both, preferred_element_type=f32)
    mine = weighted[:, :head_size]
    for k in range(1, key_heads):
        mine = jnp.where(
            head_row // groups == k, weighted[:, k * head_size : (k + 1) * head_size], mine
        )
    numerator = mine + own_weight.astype(bf16).astype(f32) * own_value
    att_buf[me] = (numerator / denominator).astype(bf16)

    pl.semaphore_wait(barrier, n - 1)
    spread(0, att_buf)

    for copy in smalls[4:]:
        copy.wait()
    route_scores = route_scores_ref[...]
    gate_weights = (
        route_scores / jnp.sum(route_scores, axis=0, keepdims=True) * routed_scale
    )
    expert_row = lax.broadcasted_iota(jnp.int32, (n, rows), 0)
    share = jnp.zeros((n, rows), f32)
    for k in range(routes_ref.shape[0]):
        share = share + jnp.where(
            routes_ref[k : k + 1] == expert_row, gate_weights[k : k + 1], 0.0
        )
    row_eye = lax.broadcasted_iota(jnp.int32, (rows, rows), 0) == lax.broadcasted_iota(
        jnp.int32, (rows, rows), 1
    )
    shares = [
        jnp.sum(jnp.where(row_eye, share[e : e + 1], 0.0), axis=1, keepdims=True)
        for e in range(n)
    ]
    out_w_copy.wait()

    arrive(0, att_buf)
    att_wide[...] = att_buf[...].astype(f32).reshape(n * heads, head_size)
    attended = jnp.concatenate(
        [att_wide[pl.ds(h, n, stride=heads), :].astype(bf16) for h in range(heads)], axis=1
    )
    mixed = jnp.dot(attended, out_w[...], preferred_element_type=f32)
    stream = (residual_ref[...].astype(f32) + mixed).astype(bf16)
    stream_buf[me] = widen(stream)
    spread(1, stream_buf)
    sgate_copy.wait()
    sup_copy.wait()
    gate_copy.wait()
    up_copy.wait()

    def here(peer):
        remote(1, stream_buf.at[peer], stream_buf.at[peer], peer, peer).wait_recv()

    weights = (sgate_w, sup_w, gate_w, up_w)
    sums = [jnp.zeros((rows, w.shape[0]), f32) for w in weights]
    squares = jnp.zeros((rows, 1), f32)
    for i in range(turns):
        c = visit(i)
        part = pl.ds(pl.multiple_of(c * wide, wide), wide)
        for t in range(per):
            peer = c * per + t
            if i:
                here(peer)
            else:
                pl.when(peer != me)(functools.partial(here, peer))
        block = join_lanes([stream_buf[c * per + t] for t in range(per)], width).astype(f32)
        squares = squares + jnp.sum(block * block, axis=1, keepdims=True)
        scaled = (block * gain_ref[:, part]).astype(bf16)
        sums = [total + dot_t(scaled, w[:, part]) for total, w in zip(sums, weights)]
    inv_rms = lax.rsqrt(squares * (1.0 / model) + norm_eps)
    sgated, supped, gated, upped = [total * inv_rms for total in sums]

    mid_buf[me] = widen((jax.nn.silu(sgated) * supped).astype(bf16))
    spread(2, mid_buf)

    hidden = (jax.nn.silu(gated) * upped).astype(bf16)
    down_copy.wait()

    def send_block(peer):
        remote(3, eo_src.at[peer], eo_buf.at[me], peer, me).start()

    for i in range(turns):
        c = visit(turns - 1 - i)
        part = pl.ds(pl.multiple_of(c * wide, wide), wide)
        out = jnp.dot(hidden, down_w[:, part], preferred_element_type=f32).astype(bf16)
        for s in range(per):
            peer = c * per + s
            eo_src[peer] = widen(out[:, s * width : (s + 1) * width])
        for s in range(per):
            peer = c * per + s
            if i < turns - 1:
                send_block(peer)
            else:
                pl.when(peer != me)(functools.partial(send_block, peer))
    eo_buf[me] = eo_src[me]

    sdown_copy.wait()
    arrive(2, mid_buf)
    mid = join_lanes([mid_buf[j] for j in range(n)], shared_width)
    total = stream.astype(f32) + jnp.dot(mid, sdown_w[...], preferred_element_type=f32)
    arrive(3, eo_buf)
    for e in range(n):
        total = total + shares[e] * eo_buf[e][:, :width].astype(f32)
    out_ref[...] = total.astype(bf16)

    sent(0, att_buf)
    sent(1, stream_buf)
    sent(2, mid_buf)
    sent(3, eo_buf)


def solution(mesh):
    n = mesh.shape["ep"]

    def on_device(
        queries,
        fresh_token_key,
        value_new,
        forget_logit,
        cache_keys,
        cache_values,
        cache_cumlog,
        lengths,
        residual,
        out_weight,
        norm_gain,
        expert_gate,
        expert_up,
        expert_down,
        shared_gate,
        shared_up,
        shared_down,
        routes,
        route_scores,
    ):
        rows, width = residual.shape
        heads, head_size = queries.shape[1:]
        span = cache_keys.shape[2]
        lanes = -(-width // LANES) * LANES
        mid_lanes = -(-shared_gate.shape[0] // LANES) * LANES
        chunks = 4
        vmem = pl.BlockSpec(memory_space=pltpu.VMEM)
        hbm = pl.BlockSpec(memory_space=pltpu.HBM)

        def like(a, drop=0):
            return pltpu.VMEM(a.shape[drop:], a.dtype)

        return pl.pallas_call(
            functools.partial(layer, n),
            out_shape=jax.ShapeDtypeStruct((rows, width), bf16),
            in_specs=[pl.BlockSpec(memory_space=pltpu.SMEM)] + [hbm] * 18,
            out_specs=vmem,
            scratch_shapes=[
                like(queries),
                like(fresh_token_key),
                like(value_new),
                like(forget_logit),
                like(residual),
                pltpu.VMEM((1, norm_gain.shape[0]), f32),
                pltpu.VMEM(routes.shape[::-1], routes.dtype),
                pltpu.VMEM(route_scores.shape[::-1], f32),
                like(cache_keys, 1),
                like(cache_values, 1),
                like(cache_cumlog, 1),
                like(out_weight),
                like(expert_gate, 1),
                like(expert_up, 1),
                like(expert_down, 1),
                like(shared_gate),
                like(shared_up),
                like(shared_down),
                pltpu.VMEM((heads, span), f32),
                pltpu.VMEM((n, heads, head_size), bf16),
                pltpu.VMEM((n * heads, head_size), f32),
                pltpu.VMEM((n, rows, lanes), bf16),
                pltpu.VMEM((n, rows, mid_lanes), bf16),
                pltpu.VMEM((n, rows, lanes), bf16),
                pltpu.VMEM((n, rows, lanes), bf16),
                pltpu.SemaphoreType.DMA((8,)),
                pltpu.SemaphoreType.DMA((8,)),
                pltpu.SemaphoreType.DMA((chunks,)),
                pltpu.SemaphoreType.DMA((chunks,)),
                pltpu.SemaphoreType.DMA((4, n)),
                pltpu.SemaphoreType.DMA((4, n)),
            ],
            compiler_params=pltpu.CompilerParams(
                collective_id=0, has_side_effects=True, vmem_limit_bytes=VMEM_LIMIT
            ),
            name="layer",
        )(
            lengths,
            queries,
            fresh_token_key,
            value_new,
            forget_logit,
            residual,
            norm_gain.reshape(1, -1),
            routes.T,
            route_scores.T,
            cache_keys,
            cache_values,
            cache_cumlog,
            out_weight,
            expert_gate,
            expert_up,
            expert_down,
            shared_gate,
            shared_up,
            shared_down,
        )

    placed = (
        P(("grp", "ep"), None, None),
        P(("grp", "ep"), None, None),
        P(("grp", "ep"), None, None),
        P(("grp", "ep"), None),
        P(("grp", "ep"), None, None, None),
        P(("grp", "ep"), None, None, None),
        P(("grp", "ep"), None, None),
        P(("grp", "ep")),
        P("grp", "ep"),
        P(None, "ep"),
        P(),
        P("ep", None, None),
        P("ep", None, None),
        P("ep", None, None),
        P("ep", None),
        P("ep", None),
        P(None, "ep"),
        P("grp", None),
        P("grp", None),
    )
    return jax.shard_map(
        on_device, mesh=mesh, in_specs=placed, out_specs=P("grp", "ep"), check_vma=False
    )
```

profile of v0, /device:TPU:0, one launch (start us, length us, event | category | flops | bytes accessed | tf_op | source)
XLA Modules:
  0.0 26.4 jit_solution(12765121696995113914)
XLA Ops:
  0.7 24.4 %layer.1 = bf16[16,128]{1,0:T(8,128)(2,1)} custom-call(s32[1]{0:T(128)S(6)} %copy.21.lengths_ref, bf16[1,8,128]{2,1,0:T(8,128)(2,1)} %q_hbm.1, bf16[1,2,128]{2,1,0:T(2,128)(2,1)} %fresh_hbm.1, bf16[1,2,128]{2,1,0:T(2,128)(2,1)} %vnew_hbm.1, f32[1,8]{1,0:T(1,128)} %forget_hbm.1, bf16[16,128]{1,0:T(8,128)(2,1)} %residual_hbm.1, f32[1,2048]{1,0:T(1,128)} %bitcast.3, ...), custom_call_target="tpu_custom_call" | custom-call | tf_op jit(solution)/shard_map/layer/pallas_call | solution.py:406
  25.1 1.3 %copy.22 = bf16[16,128]{1,0:T(8,128)(2,1)} copy(bf16[16,128]{1,0:T(8,128)(2,1)} %layer.1) | data formatting | bytes 8192
where the time goes:
time: 26.6 us; the launch traced here: 26.4 us
  Pallas kernels  24.4 us (92%)
  local copies, waits for them, and re-layouts  1.28 us (5%)
  between operations  0.66 us (2%)
    pallas_call x1, Pallas kernels, on_device(): pl.pallas_call(functools.partial(layer, n), out_shape=jax.ShapeDtypeStruc...  24.4 us
    unnamed x1, local copies, waits for them, and re-layouts  1.28 us

commit v1 on v0

v1 whole, which is shorter than its diff:
```python
import functools

import jax
import jax.numpy as jnp
from jax import lax
from jax.experimental import pallas as pl
from jax.experimental.pallas import tpu as pltpu
from jax.sharding import PartitionSpec as P

norm_eps = 1e-06
routed_scale = 2.5
contract_last = (((1,), (1,)), ((), ()))
LANES = 128
VMEM_LIMIT = 48 * 1024 * 1024
f32 = jnp.float32
bf16 = jnp.bfloat16


def dot_t(a, b):
    return lax.dot_general(a, b, contract_last, preferred_element_type=f32)


def join_lanes(blocks, width):
    if width % LANES == 0:
        return jnp.concatenate([b.astype(bf16) for b in blocks], axis=1)
    rows = blocks[0].shape[0]
    total = len(blocks) * width
    lane = lax.broadcasted_iota(jnp.int32, (rows, LANES), 1)
    pieces = [jnp.zeros((rows, LANES), f32) for _ in range(-(-total // LANES))]
    for k, block in enumerate(blocks):
        at, shift = divmod(k * width, LANES)
        moved = jnp.where(lane < width, block.astype(f32), 0.0)
        if shift:
            moved = pltpu.roll(moved, shift, 1)
        if shift + width <= LANES:
            pieces[at] = pieces[at] + moved
        else:
            pieces[at] = pieces[at] + jnp.where(lane >= shift, moved, 0.0)
            pieces[at + 1] = pieces[at + 1] + jnp.where(lane < shift, moved, 0.0)
    return jnp.concatenate([p.astype(bf16) for p in pieces], axis=1)[:, :total]


def widen(block):
    rows, width = block.shape
    short = -width % LANES
    if not short:
        return block
    return jnp.concatenate([block, jnp.zeros((rows, short), block.dtype)], axis=1)


def layer(
    n,
    lengths_hbm,
    q_hbm,
    fresh_hbm,
    vnew_hbm,
    forget_hbm,
    residual_hbm,
    gain_hbm,
    routes_hbm,
    route_scores_hbm,
    keys_hbm,
    values_hbm,
    cumlog_hbm,
    out_w_hbm,
    gate_hbm,
    up_hbm,
    down_hbm,
    sgate_hbm,
    sup_hbm,
    sdown_hbm,
    out_ref,
    lengths_ref,
    q_ref,
    fresh_ref,
    vnew_ref,
    forget_ref,
    residual_ref,
    gain_ref,
    routes_ref,
    route_scores_ref,
    keys,
    values,
    cumlog,
    out_w,
    gate_up_w,
    down_w,
    shared_w,
    sdown_w,
    att_buf,
    att_wide,
    stream_buf,
    mid_buf,
    eo_src,
    eo_buf,
    small_sem,
    load_sem,
    key_sem,
    value_sem,
    send_sem,
    recv_sem,
    stream_sem,
):
    me = lax.axis_index("ep")
    heads, head_size = q_ref.shape[1:]
    key_heads, span = keys.shape[:2]
    groups = heads // key_heads
    rows, width = residual_ref.shape
    ff, model = gate_up_w.shape[1:]
    shared_width = shared_w.shape[1]
    chunks = key_sem.shape[0]
    chunk = span // chunks

    def key_copy(c):
        part = pl.ds(c * chunk, chunk)
        return pltpu.make_async_copy(keys_hbm.at[0, :, part], keys.at[:, part], key_sem.at[c])

    def value_copy(c):
        part = pl.ds(c * chunk, chunk)
        return pltpu.make_async_copy(values_hbm.at[0, :, part], values.at[:, part], value_sem.at[c])

    cumlog_copy = pltpu.make_async_copy(cumlog_hbm.at[0], cumlog, load_sem.at[0])
    out_w_copy = pltpu.make_async_copy(out_w_hbm, out_w, load_sem.at[1])
    down_copy = pltpu.make_async_copy(down_hbm.at[0], down_w, load_sem.at[4])
    sdown_copy = pltpu.make_async_copy(sdown_hbm, sdown_w, load_sem.at[5])

    def pair_copies(first, second, both, sem):
        return [
            pltpu.make_async_copy(src, both.at[k], sem) for k, src in enumerate((first, second))
        ]

    shared_copies = pair_copies(sgate_hbm, sup_hbm, shared_w, load_sem.at[2])
    gate_up_copies = pair_copies(gate_hbm.at[0], up_hbm.at[0], gate_up_w, load_sem.at[3])

    smalls = [
        pltpu.make_async_copy(src, dst, small_sem.at[i])
        for i, (src, dst) in enumerate(
            (
                (q_hbm, q_ref),
                (fresh_hbm, fresh_ref),
                (vnew_hbm, vnew_ref),
                (forget_hbm, forget_ref),
                (lengths_hbm, lengths_ref),
                (routes_hbm, routes_ref),
                (route_scores_hbm, route_scores_ref),
                (residual_hbm, residual_ref),
                (gain_hbm, gain_ref),
            )
        )
    ]
    for copy in smalls[:5]:
        copy.start()
    cumlog_copy.start()
    for c in range(chunks):
        key_copy(c).start()
    for c in range(1):
        value_copy(c).start()

    barrier = pltpu.get_barrier_semaphore()

    def greet(i, carry):
        pl.semaphore_signal(barrier, inc=1, device_id={"ep": lax.rem(me + i, n)})
        return carry

    with jax.named_scope("greet"):
        lax.fori_loop(1, n, greet, 0)

    wide = max(width, 2 * LANES)
    per = wide // width
    turns = model // wide
    home = me // per
    toward = 1 - 2 * (home // (turns // 2))

    def remote(phase, src, dst, peer, sem):
        return pltpu.make_async_remote_copy(
            src_ref=src,
            dst_ref=dst,
            send_sem=send_sem.at[phase],
            recv_sem=sem,
            device_id={"ep": peer},
        )

    def spread(phase, buf, sem, order=""):
        def one(i, carry):
            if order == "asc":
                peer = i - 1 + (i - 1 + n - me) // n
            elif order == "desc":
                peer = n - i - jnp.where(n - i <= me, 1, 0)
            elif order == "near":
                peer = lax.rem(me + toward * i + n, n)
            else:
                peer = lax.rem(me + toward * (n - i) + n, n)
            remote(phase, buf.at[me], buf.at[me], peer, sem).start()
            return carry

        lax.fori_loop(1, n, one, 0)

    def arrive(phase, buf, sem, first, count):
        blocks = buf.at[pl.ds(first, count)]
        remote(phase, blocks, blocks, me, sem).wait_recv()

    def sent(phase, buf):
        blocks = buf.at[pl.ds(0, n - 1)]
        remote(phase, blocks, blocks, me, recv_sem.at[0]).wait_send()

    def visit(i):
        wrapped = (home + i) // turns
        return (1 - wrapped) * (home + i) + wrapped * (turns - 1 - i)

    with jax.named_scope("smallwait"):
        for copy in smalls[:5]:
            copy.wait()
    inv_root = head_size ** (-0.5)
    length = lengths_ref[0, 0]
    q = q_ref[0]
    head_row = lax.broadcasted_iota(jnp.int32, (heads, head_size), 0)
    q_wide = jnp.concatenate(
        [jnp.where(head_row // groups == k, q, jnp.zeros_like(q)) for k in range(key_heads)], axis=1
    )
    fresh, vnew = fresh_ref[0].astype(f32), vnew_ref[0].astype(f32)
    own_key, own_value = fresh[0:1], vnew[0:1]
    for k in range(1, key_heads):
        own_key = jnp.where(head_row // groups == k, fresh[k : k + 1], own_key)
        own_value = jnp.where(head_row // groups == k, vnew[k : k + 1], own_value)
    own_score = jnp.sum(q.astype(f32) * own_key, axis=1, keepdims=True) * inv_root
    eye = lax.broadcasted_iota(jnp.int32, (heads, heads), 0) == lax.broadcasted_iota(
        jnp.int32, (heads, heads), 1
    )
    forget = jnp.sum(jnp.where(eye, forget_ref[...], 0.0), axis=1, keepdims=True)
    log_gate = jnp.minimum(forget, 0.0) - jnp.log1p(jnp.exp(-jnp.abs(forget)))

    place = lax.broadcasted_iota(jnp.int32, (heads, chunk), 1)

    def both(ref, c):
        part = slice(c * chunk, (c + 1) * chunk)
        return jnp.concatenate([ref[k, part] for k in range(key_heads)], axis=1)

    def raw_score(c):
        key_copy(c).wait()
        if c + 1 < chunks:
            value_copy(c + 1).start()
        return dot_t(q_wide, both(keys, c))

    def soften(c, raw):
        score = raw * inv_root + latest - cumlog[:, c * chunk : (c + 1) * chunk]
        score = jnp.where(place + c * chunk < length, score, -jnp.inf)
        top = jnp.maximum(own_score, jnp.max(score, axis=1, keepdims=True))
        weight = jnp.exp(score - top)
        return top, jnp.sum(weight, axis=1, keepdims=True), weight.astype(bf16)

    soft = []
    with jax.named_scope("score"):
        raw = raw_score(0)
        cumlog_copy.wait()
        position = lax.broadcasted_iota(jnp.int32, (heads, span), 1)
        latest = (
            jnp.sum(jnp.where(position == length - 1, cumlog[...], 0.0), axis=1, keepdims=True)
            + log_gate
        )
        for c in range(1, chunks):
            following = raw_score(c)
            soft.append(soften(c - 1, raw))
            raw = following
        for copy in smalls[5:]:
            copy.start()
        out_w_copy.start()
    with jax.named_scope("av"):
        parts = []
        later = [[] for _ in range(chunks)]
        later[-1] = shared_copies + gate_up_copies + [down_copy, sdown_copy]
        for c in range(chunks):
            value_copy(c).wait()
            for copy in later[c]:
                copy.start()
            if c == chunks - 1:
                soft.append(soften(c, raw))
            parts.append(jnp.dot(soft[c][2], both(values, c), preferred_element_type=f32))
        top = own_score
        for chunk_top, _, _ in soft:
            top = jnp.maximum(top, chunk_top)
        own_weight = jnp.exp(own_score - top)
        denominator = own_weight
        weighted = jnp.zeros((heads, key_heads * head_size), f32)
        for (chunk_top, total, _), part in zip(soft, parts):
            scale = jnp.exp(chunk_top - top)
            denominator = denominator + scale * total
            weighted = weighted + scale * part
        mine = weighted[:, :head_size]
        for k in range(1, key_heads):
            mine = jnp.where(
                head_row // groups == k, weighted[:, k * head_size : (k + 1) * head_size], mine
            )
        numerator = mine + own_weight.astype(bf16).astype(f32) * own_value
        att_buf[me] = (numerator / denominator).astype(bf16)

    with jax.named_scope("barsend0"):
        pl.semaphore_wait(barrier, n - 1)
        spread(0, att_buf, recv_sem.at[0], '')

    with jax.named_scope("prep"):
        for copy in smalls[5:]:
            copy.wait()
        route_scores = route_scores_ref[...]
        gate_weights = (
            route_scores / jnp.sum(route_scores, axis=0, keepdims=True) * routed_scale
        )
        expert_row = lax.broadcasted_iota(jnp.int32, (n, rows), 0)
        share = jnp.zeros((n, rows), f32)
        for k in range(routes_ref.shape[0]):
            share = share + jnp.where(
                routes_ref[k : k + 1] == expert_row, gate_weights[k : k + 1], 0.0
            )
        row_eye = lax.broadcasted_iota(jnp.int32, (rows, rows), 0) == lax.broadcasted_iota(
            jnp.int32, (rows, rows), 1
        )
        shares = [
            jnp.sum(jnp.where(row_eye, share[e : e + 1], 0.0), axis=1, keepdims=True)
            for e in range(n)
        ]
        out_w_copy.wait()

    with jax.named_scope("arrive0"):
        arrive(0, att_buf, recv_sem.at[0], 0, n - 1)
    with jax.named_scope("oproj_send1"):
        att_wide[...] = att_buf[...].astype(f32).reshape(n * heads, head_size)
        attended = jnp.concatenate(
            [att_wide[pl.ds(h, n, stride=heads), :].astype(bf16) for h in range(heads)], axis=1
        )
        mixed = jnp.dot(attended, out_w[...], preferred_element_type=f32)
        stream = (residual_ref[...].astype(f32) + mixed).astype(bf16)
        stream_buf[me] = widen(stream)
        spread(1, stream_buf, stream_sem.at[home], 'desc')

    with jax.named_scope("wwait"):
        pltpu.make_async_copy(shared_w, shared_w, load_sem.at[2]).wait()
        pltpu.make_async_copy(gate_up_w, gate_up_w, load_sem.at[3]).wait()

    with jax.named_scope("gateup_send2"):
        weights = (shared_w.at[0], shared_w.at[1], gate_up_w.at[0], gate_up_w.at[1])
        sums = [jnp.zeros((rows, w.shape[0]), f32) for w in weights]
        squares = jnp.zeros((rows, 1), f32)
        for i in range(turns):
            c = visit(i)
            part = pl.ds(pl.multiple_of(c * wide, wide), wide)
            with jax.named_scope("w%d" % i):
                if i:
                    arrive(1, stream_buf, stream_sem.at[c], c * per, per)
                else:
                    arrive(1, stream_buf, stream_sem.at[c], 0, per - 1)
            block = join_lanes([stream_buf[c * per + t] for t in range(per)], width).astype(f32)
            squares = squares + jnp.sum(block * block, axis=1, keepdims=True)
            scaled = (block * gain_ref[:, part]).astype(bf16)
            sums = [total + dot_t(scaled, w[:, part]) for total, w in zip(sums, weights)]
        inv_rms = lax.rsqrt(squares * (1.0 / model) + norm_eps)
        sgated, supped, gated, upped = [total * inv_rms for total in sums]

        mid_buf[me] = widen((jax.nn.silu(sgated) * supped).astype(bf16))
        spread(2, mid_buf, recv_sem.at[1], 'asc')
        hidden = (jax.nn.silu(gated) * upped).astype(bf16)
    with jax.named_scope("down_send3"):
        down_copy.wait()

        def expert_out(i):
            part = pl.ds(i * wide, wide)
            return jnp.dot(hidden, down_w[:, part], preferred_element_type=f32).astype(bf16)

        def send_block(peer):
            remote(3, eo_src.at[peer], eo_buf.at[me], peer, recv_sem.at[2]).start()

        def put(c, out):
            for s in range(per):
                eo_src[c * per + s] = widen(out[:, s * width : (s + 1) * width])
            for s in range(per):
                peer = c * per + s
                pl.when(peer != me)(functools.partial(send_block, peer))

        out = expert_out(0)
        for i in range(1, turns):
            following = expert_out(i)
            put(i - 1, out)
            out = following
        put(turns - 1, out)
        eo_buf[me] = eo_src[me]

    with jax.named_scope("sentwait"):
        sdown_copy.wait()
        sent(0, att_buf)
        sent(1, stream_buf)
        sent(2, mid_buf)
    with jax.named_scope("arrive2"):
        arrive(2, mid_buf, recv_sem.at[1], 0, n - 1)
    with jax.named_scope("sdown"):
        mid = join_lanes([mid_buf[j] for j in range(n)], shared_width)
        total = stream.astype(f32) + jnp.dot(mid, sdown_w[...], preferred_element_type=f32)
    with jax.named_scope("arrive3"):
        sent(3, eo_src)
        arrive(3, eo_buf, recv_sem.at[2], 0, n - 1)
    with jax.named_scope("final"):
        for e in range(n):
            total = total + shares[e] * eo_buf[e][:, :width].astype(f32)
        out_ref[...] = total.astype(bf16)


def solution(mesh):
    n = mesh.shape["ep"]

    def on_device(
        queries,
        fresh_token_key,
        value_new,
        forget_logit,
        cache_keys,
        cache_values,
        cache_cumlog,
        lengths,
        residual,
        out_weight,
        norm_gain,
        expert_gate,
        expert_up,
        expert_down,
        shared_gate,
        shared_up,
        shared_down,
        routes,
        route_scores,
    ):
        rows, width = residual.shape
        heads, head_size = queries.shape[1:]
        span = cache_keys.shape[2]
        model = norm_gain.shape[0]
        lanes = -(-width // LANES) * LANES
        mid_lanes = -(-shared_gate.shape[0] // LANES) * LANES
        turns = model // max(width, 2 * LANES)
        chunks = 2
        hbm = pl.BlockSpec(memory_space=pltpu.HBM)

        def like(a, drop=0):
            return pltpu.VMEM(a.shape[drop:], a.dtype)

        def held(a):
            return pltpu.with_memory_space_constraint(a, pltpu.HBM)

        return pl.pallas_call(
            functools.partial(layer, n),
            out_shape=pltpu.VMEM((rows, width), bf16),
            in_specs=[pl.BlockSpec(memory_space=pl.ANY)] + [hbm] * 18,
            out_specs=pl.BlockSpec(memory_space=pltpu.VMEM),
            scratch_shapes=[
                pltpu.SMEM((1, 1), jnp.int32),
                like(queries),
                like(fresh_token_key),
                like(value_new),
                like(forget_logit),
                like(residual),
                pltpu.VMEM((1, model), f32),
                pltpu.VMEM(routes.shape[::-1], routes.dtype),
                pltpu.VMEM(route_scores.shape[::-1], f32),
                like(cache_keys, 1),
                like(cache_values, 1),
                like(cache_cumlog, 1),
                like(out_weight),
                pltpu.VMEM((2, *expert_gate.shape[1:]), bf16),
                like(expert_down, 1),
                pltpu.VMEM((2, *shared_gate.shape), bf16),
                like(shared_down),
                pltpu.VMEM((n, heads, head_size), bf16),
                pltpu.VMEM((n * heads, head_size), f32),
                pltpu.VMEM((n, rows, lanes), bf16),
                pltpu.VMEM((n, rows, mid_lanes), bf16),
                pltpu.VMEM((n, rows, lanes), bf16),
                pltpu.VMEM((n, rows, lanes), bf16),
                pltpu.SemaphoreType.DMA((9,)),
                pltpu.SemaphoreType.DMA((6,)),
                pltpu.SemaphoreType.DMA((chunks,)),
                pltpu.SemaphoreType.DMA((chunks,)),
                pltpu.SemaphoreType.DMA((4,)),
                pltpu.SemaphoreType.DMA((3,)),
                pltpu.SemaphoreType.DMA((turns,)),
            ],
            compiler_params=pltpu.CompilerParams(
                collective_id=0, has_side_effects=True, vmem_limit_bytes=VMEM_LIMIT
            ),
            name="layer",
        )(
            lengths.reshape(1, 1),
            *map(
                held,
                (
                    queries,
                    fresh_token_key,
                    value_new,
                    forget_logit,
                    residual,
                    norm_gain.reshape(1, -1),
                    routes.T,
                    route_scores.T,
                    cache_keys,
                    cache_values,
                    cache_cumlog,
                    out_weight,
                    expert_gate,
                    expert_up,
                    expert_down,
                    shared_gate,
                    shared_up,
                    shared_down,
                ),
            ),
        )

    placed = (
        P(("grp", "ep"), None, None),
        P(("grp", "ep"), None, None),
        P(("grp", "ep"), None, None),
        P(("grp", "ep"), None),
        P(("grp", "ep"), None, None, None),
        P(("grp", "ep"), None, None, None),
        P(("grp", "ep"), None, None),
        P(("grp", "ep")),
        P("grp", "ep"),
        P(None, "ep"),
        P(),
        P("ep", None, None),
        P("ep", None, None),
        P("ep", None, None),
        P("ep", None),
        P("ep", None),
        P(None, "ep"),
        P("grp", None),
        P("grp", None),
    )
    return jax.shard_map(
        on_device, mesh=mesh, in_specs=placed, out_specs=P("grp", "ep"), check_vma=False
    )
```

time: 26.6 us -> 21.6 us (0.81)
  Pallas kernels: 24.4 us -> 20.2 us
  local copies, waits for them, and re-layouts: 1.28 us -> 0.6 us
    pallas_call x1, Pallas kernels: 24.4 us -> 20.2 us  [on_device(): pl.pallas_call(functools.partial(layer, n), out_shape=pltpu.VMEM((rows, w...]
    unnamed x1, local copies, waits for them, and re-layouts: 1.28 us -> 0.6 us
where the time goes in v1:
time: 21.6 us; the launch traced here: 21.4 us
  Pallas kernels  20.2 us (94%)
  between operations  0.66 us (3%)
  local copies, waits for them, and re-layouts  0.6 us (3%)
    pallas_call x1, Pallas kernels, on_device(): pl.pallas_call(functools.partial(layer, n), out_shape=pltpu.VMEM((rows, w...  20.2 us
    unnamed x1, local copies, waits for them, and re-layouts  0.6 us

profile of v1, /device:TPU:0, one launch (start us, length us, event | category | flops | bytes accessed | tf_op | source)
XLA Modules:
  0.0 21.4 jit_solution(17150454651153827280)
XLA Ops:
  0.7 20.2 %layer.1 = bf16[16,128]{1,0:T(8,128)(2,1)S(1)} custom-call(s32[1,1]{1,0:T(1,128)} %bitcast.4.lengths_hbm, bf16[1,8,128]{2,1,0:T(8,128)(2,1)} %q_hbm.1, bf16[1,2,128]{2,1,0:T(2,128)(2,1)} %fresh_hbm.1, bf16[1,2,128]{2,1,0:T(2,128)(2,1)} %vnew_hbm.1, f32[1,8]{1,0:T(1,128)} %forget_hbm.1, bf16[16,128]{1,0:T(8,128)(2,1)} %residual_hbm.1, f32[1,2048]{1,0:T(1,128)} %bitcast.5, ...), custom_call_target="tpu_custom_call" | custom-call | tf_op jit(solution)/shard_map/layer/pallas_call | solution.py:444
  20.8 0.6 %copy.21 = bf16[16,128]{1,0:T(8,128)(2,1)} copy(bf16[16,128]{1,0:T(8,128)(2,1)S(1)} %layer.1) | data formatting | bytes 8192

commit v2 on v1

--- a/solution.py
+++ b/solution.py
@@ -46,6 +46,17 @@
     if not short:
         return block
     return jnp.concatenate([block, jnp.zeros((rows, short), block.dtype)], axis=1)
+
+
+def order_of(home, turns):
+    sides = 2 - turns % 2
+    row, side = divmod(home, sides)
+
+    def late(c):
+        other_row, other_side = divmod(c, sides)
+        return (c != home, 0.55 * abs(other_row - row) + 0.6 * (other_side != side) - 0.2 * other_row)
+
+    return sorted(range(turns), key=late)
 
 
 def layer(
@@ -115,14 +126,20 @@
         part = pl.ds(c * chunk, chunk)
         return pltpu.make_async_copy(keys_hbm.at[0, :, part], keys.at[:, part], key_sem.at[c])
 
+    value_parts = value_sem.shape[0]
+    late_values = 1
+    value_chunk = span // value_parts
+
     def value_copy(c):
-        part = pl.ds(c * chunk, chunk)
+        part = pl.ds(c * value_chunk, value_chunk)
         return pltpu.make_async_copy(values_hbm.at[0, :, part], values.at[:, part], value_sem.at[c])
 
     cumlog_copy = pltpu.make_async_copy(cumlog_hbm.at[0], cumlog, load_sem.at[0])
     out_w_copy = pltpu.make_async_copy(out_w_hbm, out_w, load_sem.at[1])
     down_copy = pltpu.make_async_copy(down_hbm.at[0], down_w, load_sem.at[4])
-    sdown_copy = pltpu.make_async_copy(sdown_hbm, sdown_w, load_sem.at[5])
+    sdown_copy = pltpu.make_async_copy(
+        sdown_hbm, sdown_w.at[:, pl.ds(0, sdown_hbm.shape[1])], load_sem.at[5]
+    )
 
     def pair_copies(first, second, both, sem):
         return [
@@ -153,9 +170,10 @@
     cumlog_copy.start()
     for c in range(chunks):
         key_copy(c).start()
-    for c in range(1):
+    for c in range(value_parts - late_values):
         value_copy(c).start()
 
+    sdown_w[...] = jnp.zeros_like(sdown_w)
     barrier = pltpu.get_barrier_semaphore()
 
     def greet(i, carry):
@@ -185,6 +203,7 @@
             if order == "asc":
                 peer = i - 1 + (i - 1 + n - me) // n
             elif order == "desc":
+                peer = n - i - (me + i) // n
                 peer = n - i - jnp.where(n - i <= me, 1, 0)
             elif order == "near":
                 peer = lax.rem(me + toward * i + n, n)
@@ -203,33 +222,26 @@
         blocks = buf.at[pl.ds(0, n - 1)]
         remote(phase, blocks, blocks, me, recv_sem.at[0]).wait_send()
 
+    orders = [order_of(h, turns) for h in range(turns)]
+
+    def send_mid(peer):
+        remote(2, mid_buf.at[me], mid_buf.at[me], peer, recv_sem.at[1]).start()
+
     def visit(i):
-        wrapped = (home + i) // turns
-        return (1 - wrapped) * (home + i) + wrapped * (turns - 1 - i)
-
+        place = jnp.int32(orders[0][i])
+        for h in range(1, turns):
+            place = jnp.where(home == h, orders[h][i], place)
+        return place
+
+    inv_root = head_size ** (-0.5)
+    head_row = lax.broadcasted_iota(jnp.int32, (heads, head_size), 0)
     with jax.named_scope("smallwait"):
-        for copy in smalls[:5]:
-            copy.wait()
-    inv_root = head_size ** (-0.5)
-    length = lengths_ref[0, 0]
+        smalls[0].wait()
     q = q_ref[0]
-    head_row = lax.broadcasted_iota(jnp.int32, (heads, head_size), 0)
     q_wide = jnp.concatenate(
-        [jnp.where(head_row // groups == k, q, jnp.zeros_like(q)) for k in range(key_heads)], axis=1
+        [jnp.where(head_row // groups == k, q, jnp.zeros_like(q)) for k in range(key_heads)],
+        axis=1,
     )
-    fresh, vnew = fresh_ref[0].astype(f32), vnew_ref[0].astype(f32)
-    own_key, own_value = fresh[0:1], vnew[0:1]
-    for k in range(1, key_heads):
-        own_key = jnp.where(head_row // groups == k, fresh[k : k + 1], own_key)
-        own_value = jnp.where(head_row // groups == k, vnew[k : k + 1], own_value)
-    own_score = jnp.sum(q.astype(f32) * own_key, axis=1, keepdims=True) * inv_root
-    eye = lax.broadcasted_iota(jnp.int32, (heads, heads), 0) == lax.broadcasted_iota(
-        jnp.int32, (heads, heads), 1
-    )
-    forget = jnp.sum(jnp.where(eye, forget_ref[...], 0.0), axis=1, keepdims=True)
-    log_gate = jnp.minimum(forget, 0.0) - jnp.log1p(jnp.exp(-jnp.abs(forget)))
-
-    place = lax.broadcasted_iota(jnp.int32, (heads, chunk), 1)
 
     def both(ref, c):
         part = slice(c * chunk, (c + 1) * chunk)
@@ -237,8 +249,8 @@
 
     def raw_score(c):
         key_copy(c).wait()
-        if c + 1 < chunks:
-            value_copy(c + 1).start()
+        if c < late_values:
+            value_copy(value_parts - late_values + c).start()
         return dot_t(q_wide, both(keys, c))
 
     def soften(c, raw):
@@ -248,32 +260,49 @@
         weight = jnp.exp(score - top)
         return top, jnp.sum(weight, axis=1, keepdims=True), weight.astype(bf16)
 
-    soft = []
+    raws, soft = [], []
     with jax.named_scope("score"):
-        raw = raw_score(0)
-        cumlog_copy.wait()
-        position = lax.broadcasted_iota(jnp.int32, (heads, span), 1)
-        latest = (
-            jnp.sum(jnp.where(position == length - 1, cumlog[...], 0.0), axis=1, keepdims=True)
-            + log_gate
-        )
-        for c in range(1, chunks):
-            following = raw_score(c)
-            soft.append(soften(c - 1, raw))
-            raw = following
+        for c in range(chunks):
+            raws.append(raw_score(c))
+            if c == 1:
+                for copy in smalls[1:5]:
+                    copy.wait()
+                cumlog_copy.wait()
+                length = lengths_ref[0, 0]
+                fresh, vnew = fresh_ref[0].astype(f32), vnew_ref[0].astype(f32)
+                own_key, own_value = fresh[0:1], vnew[0:1]
+                for k in range(1, key_heads):
+                    own_key = jnp.where(head_row // groups == k, fresh[k : k + 1], own_key)
+                    own_value = jnp.where(head_row // groups == k, vnew[k : k + 1], own_value)
+                own_score = jnp.sum(q.astype(f32) * own_key, axis=1, keepdims=True) * inv_root
+                eye = lax.broadcasted_iota(jnp.int32, (heads, heads), 0) == lax.broadcasted_iota(
+                    jnp.int32, (heads, heads), 1
+                )
+                forget = jnp.sum(jnp.where(eye, forget_ref[...], 0.0), axis=1, keepdims=True)
+                log_gate = jnp.minimum(forget, 0.0) - jnp.log1p(jnp.exp(-jnp.abs(forget)))
+                position = lax.broadcasted_iota(jnp.int32, (heads, span), 1)
+                latest = (
+                    jnp.sum(jnp.where(position == length - 1, cumlog[...], 0.0), axis=1, keepdims=True)
+                    + log_gate
+                )
+                place = lax.broadcasted_iota(jnp.int32, (heads, chunk), 1)
+            if c > 1:
+                while len(soft) < c:
+                    soft.append(soften(len(soft), raws[len(soft)]))
         for copy in smalls[5:]:
             copy.start()
         out_w_copy.start()
     with jax.named_scope("av"):
         parts = []
-        later = [[] for _ in range(chunks)]
-        later[-1] = shared_copies + gate_up_copies + [down_copy, sdown_copy]
         for c in range(chunks):
-            value_copy(c).wait()
-            for copy in later[c]:
-                copy.start()
-            if c == chunks - 1:
-                soft.append(soften(c, raw))
+            if c % (chunks // value_parts) == 0:
+                value_copy(c // (chunks // value_parts)).wait()
+            if c == chunks - chunks // value_parts:
+                for copy in shared_copies + gate_up_copies + [down_copy, sdown_copy]:
+                    copy.start()
+            if c == 0:
+                while len(soft) < chunks:
+                    soft.append(soften(len(soft), raws[len(soft)]))
             parts.append(jnp.dot(soft[c][2], both(values, c), preferred_element_type=f32))
         top = own_score
         for chunk_top, _, _ in soft:
@@ -355,7 +384,8 @@
         sgated, supped, gated, upped = [total * inv_rms for total in sums]
 
         mid_buf[me] = widen((jax.nn.silu(sgated) * supped).astype(bf16))
-        spread(2, mid_buf, recv_sem.at[1], 'asc')
+        for s in range(per):
+            pl.when(me != s)(functools.partial(send_mid, s))
         hidden = (jax.nn.silu(gated) * upped).astype(bf16)
     with jax.named_scope("down_send3"):
         down_copy.wait()
@@ -373,9 +403,12 @@
             for s in range(per):
                 peer = c * per + s
                 pl.when(peer != me)(functools.partial(send_block, peer))
-
-        out = expert_out(0)
-        for i in range(1, turns):
+                if c:
+                    pl.when(peer != me)(functools.partial(send_mid, peer))
+
+        put(0, expert_out(0))
+        out = expert_out(1)
+        for i in range(2, turns):
             following = expert_out(i)
             put(i - 1, out)
             out = following
@@ -390,8 +423,9 @@
     with jax.named_scope("arrive2"):
         arrive(2, mid_buf, recv_sem.at[1], 0, n - 1)
     with jax.named_scope("sdown"):
-        mid = join_lanes([mid_buf[j] for j in range(n)], shared_width)
-        total = stream.astype(f32) + jnp.dot(mid, sdown_w[...], preferred_element_type=f32)
+        mid = jnp.concatenate([mid_buf[j] for j in range(n)], axis=1)
+        shared_down = sdown_w[...].reshape(mid.shape[1], width)
+        total = stream.astype(f32) + jnp.dot(mid, shared_down, preferred_element_type=f32)
     with jax.named_scope("arrive3"):
         sent(3, eo_src)
         arrive(3, eo_buf, recv_sem.at[2], 0, n - 1)
@@ -432,7 +466,7 @@
         lanes = -(-width // LANES) * LANES
         mid_lanes = -(-shared_gate.shape[0] // LANES) * LANES
         turns = model // max(width, 2 * LANES)
-        chunks = 2
+        chunks = 4
         hbm = pl.BlockSpec(memory_space=pltpu.HBM)
 
         def like(a, drop=0):
@@ -463,7 +497,7 @@
                 pltpu.VMEM((2, *expert_gate.shape[1:]), bf16),
                 like(expert_down, 1),
                 pltpu.VMEM((2, *shared_gate.shape), bf16),
-                like(shared_down),
+                pltpu.VMEM((n, mid_lanes, width), bf16),
                 pltpu.VMEM((n, heads, head_size), bf16),
                 pltpu.VMEM((n * heads, head_size), f32),
                 pltpu.VMEM((n, rows, lanes), bf16),
@@ -473,7 +507,7 @@
                 pltpu.SemaphoreType.DMA((9,)),
                 pltpu.SemaphoreType.DMA((6,)),
                 pltpu.SemaphoreType.DMA((chunks,)),
-                pltpu.SemaphoreType.DMA((chunks,)),
+                pltpu.SemaphoreType.DMA((2,)),
                 pltpu.SemaphoreType.DMA((4,)),
                 pltpu.SemaphoreType.DMA((3,)),
                 pltpu.SemaphoreType.DMA((turns,)),
@@ -504,7 +538,7 @@
                     expert_down,
                     shared_gate,
                     shared_up,
-                    shared_down,
+                    shared_down.reshape(n, -1, width),
                 ),
             ),
         )

time: 21.6 us -> 20.8 us (0.963)
  Pallas kernels: 20.2 us -> 19.4 us
    pallas_call x1, Pallas kernels: 20.2 us -> 19.4 us  [on_device(): pl.pallas_call(functools.partial(layer, n), out_shape=pltpu.VMEM((rows, w...]
where the time goes in v2:
time: 20.8 us; the launch traced here: 20.7 us
  Pallas kernels  19.4 us (93%)
  between operations  0.66 us (3%)
  local copies, waits for them, and re-layouts  0.6 us (3%)
    pallas_call x1, Pallas kernels, on_device(): pl.pallas_call(functools.partial(layer, n), out_shape=pltpu.VMEM((rows, w...  19.4 us
    unnamed x1, local copies, waits for them, and re-layouts  0.6 us

profile of v2, /device:TPU:0, one launch (start us, length us, event | category | flops | bytes accessed | tf_op | source)
XLA Modules:
  0.0 20.7 jit_solution(2834529811599125867)
XLA Ops:
  0.7 19.4 %layer.1 = bf16[16,128]{1,0:T(8,128)(2,1)S(1)} custom-call(s32[1,1]{1,0:T(1,128)} %bitcast.5.lengths_hbm, bf16[1,8,128]{2,1,0:T(8,128)(2,1)} %q_hbm.1, bf16[1,2,128]{2,1,0:T(2,128)(2,1)} %fresh_hbm.1, bf16[1,2,128]{2,1,0:T(2,128)(2,1)} %vnew_hbm.1, f32[1,8]{1,0:T(1,128)} %forget_hbm.1, bf16[16,128]{1,0:T(8,128)(2,1)} %residual_hbm.1, f32[1,2048]{1,0:T(1,128)} %bitcast.7, ...), custom_call_target="tpu_custom_call" | custom-call | tf_op jit(solution)/shard_map/layer/pallas_call | solution.py:478
  20.1 0.6 %copy.21 = bf16[16,128]{1,0:T(8,128)(2,1)} copy(bf16[16,128]{1,0:T(8,128)(2,1)S(1)} %layer.1) | data formatting | bytes 8192

commit v3 on v2

--- a/solution.py
+++ b/solution.py
@@ -116,7 +116,7 @@
     heads, head_size = q_ref.shape[1:]
     key_heads, span = keys.shape[:2]
     groups = heads // key_heads
-    rows, width = residual_ref.shape
+    rows, width = residual_ref.shape[1:]
     ff, model = gate_up_w.shape[1:]
     shared_width = shared_w.shape[1]
     chunks = key_sem.shape[0]
@@ -135,7 +135,9 @@
         return pltpu.make_async_copy(values_hbm.at[0, :, part], values.at[:, part], value_sem.at[c])
 
     cumlog_copy = pltpu.make_async_copy(cumlog_hbm.at[0], cumlog, load_sem.at[0])
-    out_w_copy = pltpu.make_async_copy(out_w_hbm, out_w, load_sem.at[1])
+    out_w_copy = pltpu.make_async_copy(
+        out_w_hbm, out_w.at[lax.rem(me, 2)], load_sem.at[1]
+    )
     down_copy = pltpu.make_async_copy(down_hbm.at[0], down_w, load_sem.at[4])
     sdown_copy = pltpu.make_async_copy(
         sdown_hbm, sdown_w.at[:, pl.ds(0, sdown_hbm.shape[1])], load_sem.at[5]
@@ -160,31 +162,31 @@
                 (lengths_hbm, lengths_ref),
                 (routes_hbm, routes_ref),
                 (route_scores_hbm, route_scores_ref),
-                (residual_hbm, residual_ref),
+                (residual_hbm, residual_ref.at[lax.rem(me, 2)]),
                 (gain_hbm, gain_ref),
             )
         )
     ]
+    key_copy(0).start()
     for copy in smalls[:5]:
         copy.start()
     cumlog_copy.start()
-    for c in range(chunks):
+    for c in range(1, chunks):
         key_copy(c).start()
     for c in range(value_parts - late_values):
         value_copy(c).start()
-
     sdown_w[...] = jnp.zeros_like(sdown_w)
     barrier = pltpu.get_barrier_semaphore()
 
-    def greet(i, carry):
-        pl.semaphore_signal(barrier, inc=1, device_id={"ep": lax.rem(me + i, n)})
-        return carry
-
     with jax.named_scope("greet"):
-        lax.fori_loop(1, n, greet, 0)
-
-    wide = max(width, 2 * LANES)
+        for i in range(1, n):
+            pl.semaphore_signal(barrier, inc=1, device_id={"ep": lax.rem(me + i, n)})
+
+    wide = 2 * max(width, LANES)
     per = wide // width
+    pairs, pair_per = n // 2, per // 2
+    pair, side = me // 2, lax.rem(me, 2)
+    leads = side == 1
     turns = model // wide
     home = me // per
     toward = 1 - 2 * (home // (turns // 2))
@@ -198,34 +200,18 @@
             device_id={"ep": peer},
         )
 
-    def spread(phase, buf, sem, order=""):
-        def one(i, carry):
-            if order == "asc":
-                peer = i - 1 + (i - 1 + n - me) // n
-            elif order == "desc":
-                peer = n - i - (me + i) // n
-                peer = n - i - jnp.where(n - i <= me, 1, 0)
-            elif order == "near":
-                peer = lax.rem(me + toward * i + n, n)
-            else:
-                peer = lax.rem(me + toward * (n - i) + n, n)
-            remote(phase, buf.at[me], buf.at[me], peer, sem).start()
-            return carry
-
-        lax.fori_loop(1, n, one, 0)
-
     def arrive(phase, buf, sem, first, count):
         blocks = buf.at[pl.ds(first, count)]
         remote(phase, blocks, blocks, me, sem).wait_recv()
 
-    def sent(phase, buf):
-        blocks = buf.at[pl.ds(0, n - 1)]
+    def sent(phase, buf, count):
+        blocks = buf.at[pl.ds(0, count)]
         remote(phase, blocks, blocks, me, recv_sem.at[0]).wait_send()
 
     orders = [order_of(h, turns) for h in range(turns)]
 
     def send_mid(peer):
-        remote(2, mid_buf.at[me], mid_buf.at[me], peer, recv_sem.at[1]).start()
+        remote(5, mid_buf.at[me], mid_buf.at[me], peer, recv_sem.at[1]).start()
 
     def visit(i):
         place = jnp.int32(orders[0][i])
@@ -297,9 +283,6 @@
         for c in range(chunks):
             if c % (chunks // value_parts) == 0:
                 value_copy(c // (chunks // value_parts)).wait()
-            if c == chunks - chunks // value_parts:
-                for copy in shared_copies + gate_up_copies + [down_copy, sdown_copy]:
-                    copy.start()
             if c == 0:
                 while len(soft) < chunks:
                     soft.append(soften(len(soft), raws[len(soft)]))
@@ -324,11 +307,32 @@
 
     with jax.named_scope("barsend0"):
         pl.semaphore_wait(barrier, n - 1)
-        spread(0, att_buf, recv_sem.at[0], '')
-
-    with jax.named_scope("prep"):
+        def send_row(to):
+            peer = 2 * to + 1
+            remote(0, att_buf.at[me], att_buf.at[me], peer, recv_sem.at[0]).start()
+
+        outward = 1 - 2 * (pair // (pairs // 2))
+        for i in range(1, pairs):
+            send_row(lax.rem(pair + outward * (pairs - i) + pairs, pairs))
+        pl.when(side == 0)(functools.partial(send_row, pair))
+        for copy in shared_copies + gate_up_copies + [down_copy, sdown_copy]:
+            copy.start()
+
+    def lend(phase, buf, sem):
+        return remote(phase, buf.at[0], buf.at[0], me + 1 - 2 * side, sem)
+
+    lent = (lend(3, out_w, recv_sem.at[3]), lend(4, residual_ref, recv_sem.at[4]))
+    with jax.named_scope("lend"):
         for copy in smalls[5:]:
             copy.wait()
+        out_w_copy.wait()
+
+        @pl.when(side == 0)
+        def _():
+            for copy in lent:
+                copy.start()
+
+    with jax.named_scope("prep"):
         route_scores = route_scores_ref[...]
         gate_weights = (
             route_scores / jnp.sum(route_scores, axis=0, keepdims=True) * routed_scale
@@ -346,19 +350,28 @@
             jnp.sum(jnp.where(row_eye, share[e : e + 1], 0.0), axis=1, keepdims=True)
             for e in range(n)
         ]
-        out_w_copy.wait()
-
-    with jax.named_scope("arrive0"):
-        arrive(0, att_buf, recv_sem.at[0], 0, n - 1)
-    with jax.named_scope("oproj_send1"):
-        att_wide[...] = att_buf[...].astype(f32).reshape(n * heads, head_size)
-        attended = jnp.concatenate(
-            [att_wide[pl.ds(h, n, stride=heads), :].astype(bf16) for h in range(heads)], axis=1
-        )
-        mixed = jnp.dot(attended, out_w[...], preferred_element_type=f32)
-        stream = (residual_ref[...].astype(f32) + mixed).astype(bf16)
-        stream_buf[me] = widen(stream)
-        spread(1, stream_buf, stream_sem.at[home], 'desc')
+
+    def project():
+        for copy in lent:
+            copy.wait_recv()
+        with jax.named_scope("arrive0"):
+            arrive(0, att_buf, recv_sem.at[0], 0, n - 1)
+        with jax.named_scope("oproj_send1"):
+            att_wide[...] = att_buf[...].astype(f32).reshape(n * heads, head_size)
+            attended = jnp.concatenate(
+                [att_wide[pl.ds(h, n, stride=heads), :].astype(bf16) for h in range(heads)], axis=1
+            )
+            halves = []
+            for k in range(2):
+                mixed = jnp.dot(attended, out_w[k], preferred_element_type=f32)
+                halves.append(widen((residual_ref[k].astype(f32) + mixed).astype(bf16)))
+            stream_buf[pair] = widen(join_lanes(halves, width))
+            for i in range(1, n):
+                peer = n - i - jnp.where(n - i <= me, 1, 0)
+                block = stream_buf.at[pair]
+                remote(1 + lax.rem(peer, 2), block, block, peer, stream_sem.at[home]).start()
+
+    pl.when(leads)(project)
 
     with jax.named_scope("wwait"):
         pltpu.make_async_copy(shared_w, shared_w, load_sem.at[2]).wait()
@@ -372,11 +385,16 @@
             c = visit(i)
             part = pl.ds(pl.multiple_of(c * wide, wide), wide)
             with jax.named_scope("w%d" % i):
+                come = functools.partial(arrive, 1, stream_buf, stream_sem.at[c])
                 if i:
-                    arrive(1, stream_buf, stream_sem.at[c], c * per, per)
+                    come(c * pair_per, pair_per)
                 else:
-                    arrive(1, stream_buf, stream_sem.at[c], 0, per - 1)
-            block = join_lanes([stream_buf[c * per + t] for t in range(per)], width).astype(f32)
+                    pl.when(side == 0)(functools.partial(come, 0, pair_per))
+                    if pair_per > 1:
+                        pl.when(leads)(functools.partial(come, 0, pair_per - 1))
+            block = join_lanes(
+                [stream_buf[c * pair_per + t] for t in range(pair_per)], 2 * width
+            ).astype(f32)
             squares = squares + jnp.sum(block * block, axis=1, keepdims=True)
             scaled = (block * gain_ref[:, part]).astype(bf16)
             sums = [total + dot_t(scaled, w[:, part]) for total, w in zip(sums, weights)]
@@ -395,7 +413,7 @@
             return jnp.dot(hidden, down_w[:, part], preferred_element_type=f32).astype(bf16)
 
         def send_block(peer):
-            remote(3, eo_src.at[peer], eo_buf.at[me], peer, recv_sem.at[2]).start()
+            remote(6, eo_src.at[peer], eo_buf.at[me], peer, recv_sem.at[2]).start()
 
         def put(c, out):
             for s in range(per):
@@ -417,17 +435,30 @@
 
     with jax.named_scope("sentwait"):
         sdown_copy.wait()
-        sent(0, att_buf)
-        sent(1, stream_buf)
-        sent(2, mid_buf)
+
+        @pl.when(side == 0)
+        def _():
+            sent(0, att_buf, pairs)
+            for copy in lent:
+                copy.wait_send()
+
+        @pl.when(leads)
+        def _():
+            sent(0, att_buf, pairs - 1)
+            sent(1, stream_buf, pairs)
+            sent(2, stream_buf, pairs - 1)
+
+        sent(5, mid_buf, n - 1)
     with jax.named_scope("arrive2"):
         arrive(2, mid_buf, recv_sem.at[1], 0, n - 1)
     with jax.named_scope("sdown"):
         mid = jnp.concatenate([mid_buf[j] for j in range(n)], axis=1)
         shared_down = sdown_w[...].reshape(mid.shape[1], width)
-        total = stream.astype(f32) + jnp.dot(mid, shared_down, preferred_element_type=f32)
+        mine = stream_buf[pair].astype(f32)
+        stream = jnp.where(leads, mine[:, width : 2 * width], mine[:, :width])
+        total = stream + jnp.dot(mid, shared_down, preferred_element_type=f32)
     with jax.named_scope("arrive3"):
-        sent(3, eo_src)
+        sent(6, eo_src, n - 1)
         arrive(3, eo_buf, recv_sem.at[2], 0, n - 1)
     with jax.named_scope("final"):
         for e in range(n):
@@ -465,7 +496,8 @@
         model = norm_gain.shape[0]
         lanes = -(-width // LANES) * LANES
         mid_lanes = -(-shared_gate.shape[0] // LANES) * LANES
-        turns = model // max(width, 2 * LANES)
+        pair_lanes = -(-2 * width // LANES) * LANES
+        turns = model // (2 * max(width, LANES))
         chunks = 4
         hbm = pl.BlockSpec(memory_space=pltpu.HBM)
 
@@ -486,21 +518,21 @@
                 like(fresh_token_key),
                 like(value_new),
                 like(forget_logit),
-                like(residual),
+                pltpu.VMEM((2, *residual.shape), bf16),
                 pltpu.VMEM((1, model), f32),
                 pltpu.VMEM(routes.shape[::-1], routes.dtype),
                 pltpu.VMEM(route_scores.shape[::-1], f32),
                 like(cache_keys, 1),
                 like(cache_values, 1),
                 like(cache_cumlog, 1),
-                like(out_weight),
+                pltpu.VMEM((2, *out_weight.shape), bf16),
                 pltpu.VMEM((2, *expert_gate.shape[1:]), bf16),
                 like(expert_down, 1),
                 pltpu.VMEM((2, *shared_gate.shape), bf16),
                 pltpu.VMEM((n, mid_lanes, width), bf16),
                 pltpu.VMEM((n, heads, head_size), bf16),
                 pltpu.VMEM((n * heads, head_size), f32),
-                pltpu.VMEM((n, rows, lanes), bf16),
+                pltpu.VMEM((n // 2, rows, pair_lanes), bf16),
                 pltpu.VMEM((n, rows, mid_lanes), bf16),
                 pltpu.VMEM((n, rows, lanes), bf16),
                 pltpu.VMEM((n, rows, lanes), bf16),
@@ -508,8 +540,8 @@
                 pltpu.SemaphoreType.DMA((6,)),
                 pltpu.SemaphoreType.DMA((chunks,)),
                 pltpu.SemaphoreType.DMA((2,)),
-                pltpu.SemaphoreType.DMA((4,)),
-                pltpu.SemaphoreType.DMA((3,)),
+                pltpu.SemaphoreType.DMA((7,)),
+                pltpu.SemaphoreType.DMA((5,)),
                 pltpu.SemaphoreType.DMA((turns,)),
             ],
             compiler_params=pltpu.CompilerParams(

time: 20.8 us -> 20.1 us (0.966)
  Pallas kernels: 19.4 us -> 18.7 us
    pallas_call x1, Pallas kernels: 19.4 us -> 18.7 us  [on_device(): pl.pallas_call(functools.partial(layer, n), out_shape=pltpu.VMEM((rows, w...]
where the time goes in v3:
time: 20.1 us; the launch traced here: 19.9 us
  Pallas kernels  18.7 us (93%)
  between operations  0.66 us (3%)
  local copies, waits for them, and re-layouts  0.6 us (3%)
    pallas_call x1, Pallas kernels, on_device(): pl.pallas_call(functools.partial(layer, n), out_shape=pltpu.VMEM((rows, w...  18.7 us
    unnamed x1, local copies, waits for them, and re-layouts  0.6 us

profile of v3, /device:TPU:0, one launch (start us, length us, event | category | flops | bytes accessed | tf_op | source)
XLA Modules:
  0.0 19.9 jit_solution(16458396824404396105)
XLA Ops:
  0.7 18.7 %layer.1 = bf16[16,128]{1,0:T(8,128)(2,1)S(1)} custom-call(s32[1,1]{1,0:T(1,128)} %bitcast.5.lengths_hbm, bf16[1,8,128]{2,1,0:T(8,128)(2,1)} %q_hbm.1, bf16[1,2,128]{2,1,0:T(2,128)(2,1)} %fresh_hbm.1, bf16[1,2,128]{2,1,0:T(2,128)(2,1)} %vnew_hbm.1, f32[1,8]{1,0:T(1,128)} %forget_hbm.1, bf16[16,128]{1,0:T(8,128)(2,1)} %residual_hbm.1, f32[1,2048]{1,0:T(1,128)} %bitcast.7, ...), custom_call_target="tpu_custom_call" | custom-call | tf_op jit(solution)/shard_map/layer/pallas_call | solution.py:510
  19.3 0.6 %copy.21 = bf16[16,128]{1,0:T(8,128)(2,1)} copy(bf16[16,128]{1,0:T(8,128)(2,1)S(1)} %layer.1) | data formatting | bytes 8192

commit v4 on v3

--- a/solution.py
+++ b/solution.py
@@ -48,15 +48,30 @@
     return jnp.concatenate([block, jnp.zeros((rows, short), block.dtype)], axis=1)
 
 
-def order_of(home, turns):
+def hops(a, b, sides):
+    return abs(a // sides - b // sides) + (a % sides != b % sides)
+
+
+def visit_order(home, turns):
     sides = 2 - turns % 2
-    row, side = divmod(home, sides)
 
     def late(c):
-        other_row, other_side = divmod(c, sides)
-        return (c != home, 0.55 * abs(other_row - row) + 0.6 * (other_side != side) - 0.2 * other_row)
+        sent = max(hops(c, turns - 1, sides), hops(c, 0, sides) - 1)
+        return (c != home, 0.55 * abs(c // sides - home // sides) + 0.6 * (c % sides != home % sides) - 0.2 * (c // sides))
 
     return sorted(range(turns), key=late)
+
+
+def send_order(home, pairs):
+    sides = 2 - pairs % 2
+    return sorted((c for c in range(pairs) if c != home), key=lambda c: -c)
+
+
+def pick(table, at):
+    entry = jnp.int32(table[0])
+    for h in range(1, len(table)):
+        entry = jnp.where(at == h, table[h], entry)
+    return entry
 
 
 def layer(
@@ -104,8 +119,9 @@
     mid_buf,
     eo_src,
     eo_buf,
+    first_shared,
+    first_expert,
     small_sem,
-    load_sem,
     key_sem,
     value_sem,
     send_sem,
@@ -126,7 +142,7 @@
         part = pl.ds(c * chunk, chunk)
         return pltpu.make_async_copy(keys_hbm.at[0, :, part], keys.at[:, part], key_sem.at[c])
 
-    value_parts = value_sem.shape[0]
+    value_parts = value_sem.shape[0] - 1
     late_values = 1
     value_chunk = span // value_parts
 
@@ -134,13 +150,13 @@
         part = pl.ds(c * value_chunk, value_chunk)
         return pltpu.make_async_copy(values_hbm.at[0, :, part], values.at[:, part], value_sem.at[c])
 
-    cumlog_copy = pltpu.make_async_copy(cumlog_hbm.at[0], cumlog, load_sem.at[0])
+    cumlog_copy = pltpu.make_async_copy(cumlog_hbm.at[0], cumlog, value_sem.at[2])
     out_w_copy = pltpu.make_async_copy(
-        out_w_hbm, out_w.at[lax.rem(me, 2)], load_sem.at[1]
+        out_w_hbm, out_w.at[lax.rem(me, 2)], key_sem.at[1]
     )
-    down_copy = pltpu.make_async_copy(down_hbm.at[0], down_w, load_sem.at[4])
+    down_copy = pltpu.make_async_copy(down_hbm.at[0], down_w, key_sem.at[0])
     sdown_copy = pltpu.make_async_copy(
-        sdown_hbm, sdown_w.at[:, pl.ds(0, sdown_hbm.shape[1])], load_sem.at[5]
+        sdown_hbm, sdown_w.at[:, pl.ds(0, sdown_hbm.shape[1])], small_sem.at[4]
     )
 
     def pair_copies(first, second, both, sem):
@@ -148,11 +164,11 @@
             pltpu.make_async_copy(src, both.at[k], sem) for k, src in enumerate((first, second))
         ]
 
-    shared_copies = pair_copies(sgate_hbm, sup_hbm, shared_w, load_sem.at[2])
-    gate_up_copies = pair_copies(gate_hbm.at[0], up_hbm.at[0], gate_up_w, load_sem.at[3])
+    shared_copies = pair_copies(sgate_hbm, sup_hbm, shared_w, key_sem.at[2])
+    gate_up_copies = pair_copies(gate_hbm.at[0], up_hbm.at[0], gate_up_w, key_sem.at[3])
 
     smalls = [
-        pltpu.make_async_copy(src, dst, small_sem.at[i])
+        pltpu.make_async_copy(src, dst, small_sem.at[i % 5])
         for i, (src, dst) in enumerate(
             (
                 (q_hbm, q_ref),
@@ -208,16 +224,15 @@
         blocks = buf.at[pl.ds(0, count)]
         remote(phase, blocks, blocks, me, recv_sem.at[0]).wait_send()
 
-    orders = [order_of(h, turns) for h in range(turns)]
-
-    def send_mid(peer):
-        remote(5, mid_buf.at[me], mid_buf.at[me], peer, recv_sem.at[1]).start()
+    visits = [visit_order(h, turns) for h in range(turns)]
+    targets = [send_order(h, pairs) for h in range(pairs)]
 
     def visit(i):
-        place = jnp.int32(orders[0][i])
-        for h in range(1, turns):
-            place = jnp.where(home == h, orders[h][i], place)
-        return place
+        return pick([order[i] for order in visits], home)
+
+    def send_mid(k):
+        peer = k + jnp.where(me <= k, 1, 0)
+        remote(0, mid_buf.at[me], mid_buf.at[me], peer, recv_sem.at[0]).start()
 
     inv_root = head_size ** (-0.5)
     head_row = lax.broadcasted_iota(jnp.int32, (heads, head_size), 0)
@@ -321,7 +336,7 @@
     def lend(phase, buf, sem):
         return remote(phase, buf.at[0], buf.at[0], me + 1 - 2 * side, sem)
 
-    lent = (lend(3, out_w, recv_sem.at[3]), lend(4, residual_ref, recv_sem.at[4]))
+    lent = (lend(1, out_w, recv_sem.at[1]), lend(2, residual_ref, recv_sem.at[2]))
     with jax.named_scope("lend"):
         for copy in smalls[5:]:
             copy.wait()
@@ -366,21 +381,39 @@
                 mixed = jnp.dot(attended, out_w[k], preferred_element_type=f32)
                 halves.append(widen((residual_ref[k].astype(f32) + mixed).astype(bf16)))
             stream_buf[pair] = widen(join_lanes(halves, width))
-            for i in range(1, n):
-                peer = n - i - jnp.where(n - i <= me, 1, 0)
-                block = stream_buf.at[pair]
-                remote(1 + lax.rem(peer, 2), block, block, peer, stream_sem.at[home]).start()
+            block = stream_buf.at[pair]
+
+            def send_stream(to, core):
+                remote(1 + core, block, block, 2 * to + core, stream_sem.at[home]).start()
+
+            send_stream(pair, 0)
+            for i in range(pairs - 1):
+                to = pick([order[i] for order in targets], pair)
+                for core in range(2):
+                    send_stream(to, core)
 
     pl.when(leads)(project)
 
+    @pl.when(side == 0)
+    def _():
+        sent(0, att_buf, pairs)
+        for copy in lent:
+            copy.wait_send()
+
+    def stream_sent():
+        sent(0, att_buf, pairs - 1)
+        sent(1, stream_buf, pairs)
+        sent(2, stream_buf, pairs - 1)
+
     with jax.named_scope("wwait"):
-        pltpu.make_async_copy(shared_w, shared_w, load_sem.at[2]).wait()
-        pltpu.make_async_copy(gate_up_w, gate_up_w, load_sem.at[3]).wait()
+        pltpu.make_async_copy(shared_w, shared_w, key_sem.at[2]).wait()
+        pltpu.make_async_copy(gate_up_w, gate_up_w, key_sem.at[3]).wait()
 
     with jax.named_scope("gateup_send2"):
         weights = (shared_w.at[0], shared_w.at[1], gate_up_w.at[0], gate_up_w.at[1])
         sums = [jnp.zeros((rows, w.shape[0]), f32) for w in weights]
         squares = jnp.zeros((rows, 1), f32)
+        firsts = (first_shared.at[0], first_shared.at[1], first_expert.at[0], first_expert.at[1])
         for i in range(turns):
             c = visit(i)
             part = pl.ds(pl.multiple_of(c * wide, wide), wide)
@@ -398,59 +431,58 @@
             squares = squares + jnp.sum(block * block, axis=1, keepdims=True)
             scaled = (block * gain_ref[:, part]).astype(bf16)
             sums = [total + dot_t(scaled, w[:, part]) for total, w in zip(sums, weights)]
+            if i == turns - 2:
+                pl.when(leads)(stream_sent)
+            if i == 0:
+                for ref, total in zip(firsts, sums):
+                    ref[...] = total
+                sums = [jnp.zeros_like(total) for total in sums]
+        sums = [ref[...] + total for ref, total in zip(firsts, sums)]
         inv_rms = lax.rsqrt(squares * (1.0 / model) + norm_eps)
         sgated, supped, gated, upped = [total * inv_rms for total in sums]
 
         mid_buf[me] = widen((jax.nn.silu(sgated) * supped).astype(bf16))
-        for s in range(per):
-            pl.when(me != s)(functools.partial(send_mid, s))
+        for k in range(per):
+            send_mid(k)
         hidden = (jax.nn.silu(gated) * upped).astype(bf16)
     with jax.named_scope("down_send3"):
         down_copy.wait()
 
-        def expert_out(i):
-            part = pl.ds(i * wide, wide)
+        def expert_out(c):
+            part = pl.ds(pl.multiple_of(c * wide, wide), wide)
             return jnp.dot(hidden, down_w[:, part], preferred_element_type=f32).astype(bf16)
 
         def send_block(peer):
-            remote(6, eo_src.at[peer], eo_buf.at[me], peer, recv_sem.at[2]).start()
-
-        def put(c, out):
+            remote(1, eo_src.at[peer], eo_buf.at[me], peer, recv_sem.at[1]).start()
+
+        def put(i, c, out):
             for s in range(per):
                 eo_src[c * per + s] = widen(out[:, s * width : (s + 1) * width])
-            for s in range(per):
-                peer = c * per + s
-                pl.when(peer != me)(functools.partial(send_block, peer))
-                if c:
-                    pl.when(peer != me)(functools.partial(send_mid, peer))
-
-        put(0, expert_out(0))
-        out = expert_out(1)
+            if i < turns - 1:
+                for s in range(per):
+                    send_block(c * per + s)
+            else:
+                for s in range(per - 1):
+                    send_block(c * per + s + jnp.where(me - c * per <= s, 1, 0))
+            if i:
+                for k in range(i * per, min((i + 1) * per, n - 1)):
+                    send_mid(k)
+
+        chips = [i + jnp.where(home <= i, 1, 0) for i in range(turns - 1)] + [home]
+        put(0, chips[0], expert_out(chips[0]))
+        out = expert_out(chips[1])
         for i in range(2, turns):
-            following = expert_out(i)
-            put(i - 1, out)
+            following = expert_out(chips[i])
+            put(i - 1, chips[i - 1], out)
             out = following
-        put(turns - 1, out)
+        put(turns - 1, home, out)
         eo_buf[me] = eo_src[me]
 
     with jax.named_scope("sentwait"):
         sdown_copy.wait()
-
-        @pl.when(side == 0)
-        def _():
-            sent(0, att_buf, pairs)
-            for copy in lent:
-                copy.wait_send()
-
-        @pl.when(leads)
-        def _():
-            sent(0, att_buf, pairs - 1)
-            sent(1, stream_buf, pairs)
-            sent(2, stream_buf, pairs - 1)
-
-        sent(5, mid_buf, n - 1)
+        sent(0, mid_buf, n - 1)
     with jax.named_scope("arrive2"):
-        arrive(2, mid_buf, recv_sem.at[1], 0, n - 1)
+        arrive(0, mid_buf, recv_sem.at[0], 0, n - 1)
     with jax.named_scope("sdown"):
         mid = jnp.concatenate([mid_buf[j] for j in range(n)], axis=1)
         shared_down = sdown_w[...].reshape(mid.shape[1], width)
@@ -458,8 +490,8 @@
         stream = jnp.where(leads, mine[:, width : 2 * width], mine[:, :width])
         total = stream + jnp.dot(mid, shared_down, preferred_element_type=f32)
     with jax.named_scope("arrive3"):
-        sent(6, eo_src, n - 1)
-        arrive(3, eo_buf, recv_sem.at[2], 0, n - 1)
+        sent(1, eo_src, n - 1)
+        arrive(1, eo_buf, recv_sem.at[1], 0, n - 1)
     with jax.named_scope("final"):
         for e in range(n):
             total = total + shares[e] * eo_buf[e][:, :width].astype(f32)
@@ -536,12 +568,13 @@
                 pltpu.VMEM((n, rows, mid_lanes), bf16),
                 pltpu.VMEM((n, rows, lanes), bf16),
                 pltpu.VMEM((n, rows, lanes), bf16),
-                pltpu.SemaphoreType.DMA((9,)),
-                pltpu.SemaphoreType.DMA((6,)),
+                pltpu.VMEM((2, rows, shared_gate.shape[0]), f32),
+                pltpu.VMEM((2, rows, expert_gate.shape[1]), f32),
+                pltpu.SemaphoreType.DMA((5,)),
                 pltpu.SemaphoreType.DMA((chunks,)),
-                pltpu.SemaphoreType.DMA((2,)),
-                pltpu.SemaphoreType.DMA((7,)),
-                pltpu.SemaphoreType.DMA((5,)),
+                pltpu.SemaphoreType.DMA((2 + 1,)),
+                pltpu.SemaphoreType.DMA((3,)),
+                pltpu.SemaphoreType.DMA((3,)),
                 pltpu.SemaphoreType.DMA((turns,)),
             ],
             compiler_params=pltpu.CompilerParams(

time: 20.1 us -> 19.9 us (0.990)
    pallas_call x1, Pallas kernels: 18.7 us -> 18.5 us  [on_device(): pl.pallas_call(functools.partial(layer, n), out_shape=pltpu.VMEM((rows, w...]
where the time goes in v4:
time: 19.9 us; the launch traced here: 19.7 us
  Pallas kernels  18.5 us (93%)
  between operations  0.66 us (3%)
  local copies, waits for them, and re-layouts  0.6 us (3%)
    pallas_call x1, Pallas kernels, on_device(): pl.pallas_call(functools.partial(layer, n), out_shape=pltpu.VMEM((rows, w...  18.5 us
    unnamed x1, local copies, waits for them, and re-layouts  0.6 us

profile of v4, /device:TPU:0, one launch (start us, length us, event | category | flops | bytes accessed | tf_op | source)
XLA Modules:
  0.0 19.7 jit_solution(7771265609232323450)
XLA Ops:
  0.7 18.5 %layer.1 = bf16[16,128]{1,0:T(8,128)(2,1)S(1)} custom-call(s32[1,1]{1,0:T(1,128)} %bitcast.5.lengths_hbm, bf16[1,8,128]{2,1,0:T(8,128)(2,1)} %q_hbm.1, bf16[1,2,128]{2,1,0:T(2,128)(2,1)} %fresh_hbm.1, bf16[1,2,128]{2,1,0:T(2,128)(2,1)} %vnew_hbm.1, f32[1,8]{1,0:T(1,128)} %forget_hbm.1, bf16[16,128]{1,0:T(8,128)(2,1)} %residual_hbm.1, f32[1,2048]{1,0:T(1,128)} %bitcast.7, ...), custom_call_target="tpu_custom_call" | custom-call | tf_op jit(solution)/shard_map/layer/pallas_call | solution.py:542
  19.1 0.6 %copy.21 = bf16[16,128]{1,0:T(8,128)(2,1)} copy(bf16[16,128]{1,0:T(8,128)(2,1)S(1)} %layer.1) | data formatting | bytes 8192

commit v5 on v4

--- a/solution.py
+++ b/solution.py
@@ -418,6 +418,9 @@
             c = visit(i)
             part = pl.ds(pl.multiple_of(c * wide, wide), wide)
             with jax.named_scope("w%d" % i):
+                if i == turns - 2:
+                    down_copy.wait()
+                    sdown_copy.wait()
                 come = functools.partial(arrive, 1, stream_buf, stream_sem.at[c])
                 if i:
                     come(c * pair_per, pair_per)
@@ -446,7 +449,6 @@
             send_mid(k)
         hidden = (jax.nn.silu(gated) * upped).astype(bf16)
     with jax.named_scope("down_send3"):
-        down_copy.wait()
 
         def expert_out(c):
             part = pl.ds(pl.multiple_of(c * wide, wide), wide)
@@ -479,7 +481,6 @@
         eo_buf[me] = eo_src[me]
 
     with jax.named_scope("sentwait"):
-        sdown_copy.wait()
         sent(0, mid_buf, n - 1)
     with jax.named_scope("arrive2"):
         arrive(0, mid_buf, recv_sem.at[0], 0, n - 1)

time: 19.9 us -> 19.8 us (level)
  no operation moved by 1% of the time
where the time goes in v5:
time: 19.8 us; the launch traced here: 19.6 us
  Pallas kernels  18.4 us (93%)
  between operations  0.66 us (3%)
  local copies, waits for them, and re-layouts  0.6 us (3%)
    pallas_call x1, Pallas kernels, on_device(): pl.pallas_call(functools.partial(layer, n), out_shape=pltpu.VMEM((rows, w...  18.4 us
    unnamed x1, local copies, waits for them, and re-layouts  0.6 us

profile of v5, /device:TPU:0, one launch (start us, length us, event | category | flops | bytes accessed | tf_op | source)
XLA Modules:
  0.0 19.6 jit_solution(18140789891936418541)
XLA Ops:
  0.7 18.4 %layer.1 = bf16[16,128]{1,0:T(8,128)(2,1)S(1)} custom-call(s32[1,1]{1,0:T(1,128)} %bitcast.5.lengths_hbm, bf16[1,8,128]{2,1,0:T(8,128)(2,1)} %q_hbm.1, bf16[1,2,128]{2,1,0:T(2,128)(2,1)} %fresh_hbm.1, bf16[1,2,128]{2,1,0:T(2,128)(2,1)} %vnew_hbm.1, f32[1,8]{1,0:T(1,128)} %forget_hbm.1, bf16[16,128]{1,0:T(8,128)(2,1)} %residual_hbm.1, f32[1,2048]{1,0:T(1,128)} %bitcast.7, ...), custom_call_target="tpu_custom_call" | custom-call | tf_op jit(solution)/shard_map/layer/pallas_call | solution.py:543
  19.0 0.6 %copy.21 = bf16[16,128]{1,0:T(8,128)(2,1)} copy(bf16[16,128]{1,0:T(8,128)(2,1)S(1)} %layer.1) | data formatting | bytes 8192

commit v6 on v5

--- a/solution.py
+++ b/solution.py
@@ -60,11 +60,6 @@
         return (c != home, 0.55 * abs(c // sides - home // sides) + 0.6 * (c % sides != home % sides) - 0.2 * (c // sides))
 
     return sorted(range(turns), key=late)
-
-
-def send_order(home, pairs):
-    sides = 2 - pairs % 2
-    return sorted((c for c in range(pairs) if c != home), key=lambda c: -c)
 
 
 def pick(table, at):
@@ -184,19 +179,20 @@
         )
     ]
     key_copy(0).start()
-    for copy in smalls[:5]:
+    smalls[0].start()
+    sdown_w[...] = jnp.zeros_like(sdown_w)
+    barrier = pltpu.get_barrier_semaphore()
+
+    with jax.named_scope("greet"):
+        for i in range(1, n):
+            pl.semaphore_signal(barrier, inc=1, device_id={"ep": lax.rem(me + i, n)})
+    for copy in smalls[1:5]:
         copy.start()
     cumlog_copy.start()
     for c in range(1, chunks):
         key_copy(c).start()
     for c in range(value_parts - late_values):
         value_copy(c).start()
-    sdown_w[...] = jnp.zeros_like(sdown_w)
-    barrier = pltpu.get_barrier_semaphore()
-
-    with jax.named_scope("greet"):
-        for i in range(1, n):
-            pl.semaphore_signal(barrier, inc=1, device_id={"ep": lax.rem(me + i, n)})
 
     wide = 2 * max(width, LANES)
     per = wide // width
@@ -225,7 +221,6 @@
         remote(phase, blocks, blocks, me, recv_sem.at[0]).wait_send()
 
     visits = [visit_order(h, turns) for h in range(turns)]
-    targets = [send_order(h, pairs) for h in range(pairs)]
 
     def visit(i):
         return pick([order[i] for order in visits], home)
@@ -386,11 +381,12 @@
             def send_stream(to, core):
                 remote(1 + core, block, block, 2 * to + core, stream_sem.at[home]).start()
 
-            send_stream(pair, 0)
             for i in range(pairs - 1):
-                to = pick([order[i] for order in targets], pair)
+                last = pairs - 1 - i
                 for core in range(2):
-                    send_stream(to, core)
+                    send_stream(last - jnp.where(last <= pair, 1, 0), core)
+                if i == 0:
+                    send_stream(pair, 0)
 
     pl.when(leads)(project)
 
@@ -480,8 +476,6 @@
         put(turns - 1, home, out)
         eo_buf[me] = eo_src[me]
 
-    with jax.named_scope("sentwait"):
-        sent(0, mid_buf, n - 1)
     with jax.named_scope("arrive2"):
         arrive(0, mid_buf, recv_sem.at[0], 0, n - 1)
     with jax.named_scope("sdown"):
@@ -491,12 +485,13 @@
         stream = jnp.where(leads, mine[:, width : 2 * width], mine[:, :width])
         total = stream + jnp.dot(mid, shared_down, preferred_element_type=f32)
     with jax.named_scope("arrive3"):
-        sent(1, eo_src, n - 1)
         arrive(1, eo_buf, recv_sem.at[1], 0, n - 1)
     with jax.named_scope("final"):
         for e in range(n):
             total = total + shares[e] * eo_buf[e][:, :width].astype(f32)
         out_ref[...] = total.astype(bf16)
+        sent(0, mid_buf, n - 1)
+        sent(1, eo_src, n - 1)
 
 
 def solution(mesh):

time: 19.8 us -> 19.8 us (level)
  no operation moved by 1% of the time
where the time goes in v6:
time: 19.8 us; the launch traced here: 19.6 us
  Pallas kernels  18.4 us (93%)
  between operations  0.66 us (3%)
  local copies, waits for them, and re-layouts  0.6 us (3%)
    pallas_call x1, Pallas kernels, on_device(): pl.pallas_call(functools.partial(layer, n), out_shape=pltpu.VMEM((rows, w...  18.4 us
    unnamed x1, local copies, waits for them, and re-layouts  0.6 us

profile of v6, /device:TPU:0, one launch (start us, length us, event | category | flops | bytes accessed | tf_op | source)
XLA Modules:
  0.0 19.6 jit_solution(12451597690641494711)
XLA Ops:
  0.7 18.4 %layer.1 = bf16[16,128]{1,0:T(8,128)(2,1)S(1)} custom-call(s32[1,1]{1,0:T(1,128)} %bitcast.5.lengths_hbm, bf16[1,8,128]{2,1,0:T(8,128)(2,1)} %q_hbm.1, bf16[1,2,128]{2,1,0:T(2,128)(2,1)} %fresh_hbm.1, bf16[1,2,128]{2,1,0:T(2,128)(2,1)} %vnew_hbm.1, f32[1,8]{1,0:T(1,128)} %forget_hbm.1, bf16[16,128]{1,0:T(8,128)(2,1)} %residual_hbm.1, f32[1,2048]{1,0:T(1,128)} %bitcast.7, ...), custom_call_target="tpu_custom_call" | custom-call | tf_op jit(solution)/shard_map/layer/pallas_call | solution.py:538
  19.0 0.6 %copy.21 = bf16[16,128]{1,0:T(8,128)(2,1)} copy(bf16[16,128]{1,0:T(8,128)(2,1)S(1)} %layer.1) | data formatting | bytes 8192
